TPU v7x, 32 devices: a whole 2x2x4 slice. The times are simulated.
32 devices in a mesh: ep: 16 (over z, y, x), tp: 2 (over core).
Axes of the slice: x: 2, y: 2, z: 4, core: 2. Of those that a mesh axis runs over, the one named last changes fastest.
Arguments:
- inputs: bfloat16 [256, 2048], P('ep'), may hold values from -6 to 6
- positions: int32 [256], P('ep'), may hold values from 1024 to 8191
- ret_state: float32 [256, 12, 128, 128], P('ep', 'tp'), may hold values from -4 to 4
- norm_mix: bfloat16 [2048], replicated, may hold values from 0.099609375 to 1.8984375
- w_query: bfloat16 [2048, 1536], P('ep', 'tp'), may hold values from -0.1875 to 0.1875
- w_key: bfloat16 [2048, 1536], P('ep', 'tp'), may hold values from -0.1875 to 0.1875
- w_value: bfloat16 [2048, 1536], P('ep', 'tp'), may hold values from -0.1875 to 0.1875
- w_gate_in: bfloat16 [2048, 1536], P('ep', 'tp'), may hold values from -0.1875 to 0.1875
- head_gain: bfloat16 [1536], P('tp'), may hold values from 0.099609375 to 1.8984375
- w_out: bfloat16 [1536, 2048], P('tp', 'ep'), may hold values from -0.15625 to 0.15625
- norm_ffn: bfloat16 [2048], replicated, may hold values from 0.099609375 to 1.8984375
- route_ids: int32 [256, 4], P('ep'), may hold values from 0 to 15, all different within a row; in each aligned block of 16 rows (0 to 15, 16 to 31, ...) at most 8 rows name the same one
- route_weight: bfloat16 [256, 4], P('ep'), may hold values from 0.19921875 to 1
- exp_gate: bfloat16 [16, 2048, 1024], P('ep', None, 'tp'), may hold values from -0.125 to 0.125
- exp_up: bfloat16 [16, 2048, 1024], P('ep', None, 'tp'), may hold values from -0.125 to 0.125
- exp_down: bfloat16 [16, 1024, 2048], P('ep', 'tp'), may hold values from -0.1875 to 0.1875
- dense_gate: bfloat16 [2048, 4096], P(None, ('ep', 'tp')), may hold values from -0.125 to 0.125
- dense_up: bfloat16 [2048, 4096], P(None, ('ep', 'tp')), may hold values from -0.125 to 0.125
- dense_down: bfloat16 [4096, 2048], P(('ep', 'tp')), may hold values from -0.1875 to 0.1875
- branch_gate: bfloat16 [2048], replicated, may hold values from -0.125 to 0.125
Outputs:
- layer_out: bfloat16 [256, 2048], P('ep')
- new_state: float32 [256, 12, 128, 128], P('ep', 'tp')
Inputs may be any that keep to these rules, and one draw needn't show every extreme that they name: `route_ids`: each row names 4 different experts. Among the rows of one index of ep no expert is named more than 8 times, a bound that some block reaches.
All inputs are finite; a program needn't handle non-finite values.
Results may differ from a plain program's by a relative error of at most 0.015.
Values may be sent and summed in bfloat16 or wider, within the bound.
A program may use at most 128 MiB of HBM per device.

v0:
```python
import jax
import jax.numpy as jnp
from jax import lax
from jax.sharding import PartitionSpec as P

D = 2048
HEADS = 12
EPS = 1e-06


def rms_scale(values, scales):
    widened = values.astype(jnp.float32)
    scaled = widened * lax.rsqrt(jnp.mean(widened * widened, axis=-1, keepdims=True) + EPS)
    return (scaled * scales.astype(jnp.float32)).astype(jnp.bfloat16)


def rotary_angles(positions, head_dim):
    halfway = head_dim // 2
    frequency = 10000.0 ** (-jnp.arange(halfway, dtype=jnp.float32) * 2.0 / head_dim)
    return positions.astype(jnp.float32)[:, None] * frequency[None, :]


def rotate_heads(values, angles):
    halfway = values.shape[-1] // 2
    cosine = jnp.cos(angles)[:, None, :]
    sine_of = jnp.sin(angles)[:, None, :]
    leading = values[..., :halfway]
    trailing = values[..., halfway:]
    return jnp.concatenate(
        [leading * cosine - trailing * sine_of, trailing * cosine + leading * sine_of], axis=-1
    )


def log_decay(head_count):
    spread = jnp.arange(head_count, dtype=jnp.float32) * (5.0 / max(head_count - 1, 1))
    return jnp.log1p(-(2.0 ** (-5.0 - spread)))


def retain(queries, keys_in, values_in, gate_pre, old_state, positions, scales, log_gamma):
    row_count, head_count, head_dim = (old_state.shape[0], old_state.shape[1], old_state.shape[2])
    angles = rotary_angles(positions, head_dim)
    rot_query = rotate_heads(
        queries.astype(jnp.float32).reshape(row_count, head_count, head_dim), angles
    )
    rot_key = rotate_heads(
        keys_in.astype(jnp.float32).reshape(row_count, head_count, head_dim), angles
    ) * head_dim ** (-0.5)
    value_heads = values_in.astype(jnp.float32).reshape(row_count, head_count, head_dim)
    new_state = (
        jnp.exp(log_gamma)[None, :, None, None] * old_state
        + rot_key[:, :, :, None] * value_heads[:, :, None, :]
    )
    readout = jnp.einsum("shd,shdv->shv", rot_query, new_state, precision=lax.Precision.HIGHEST)
    centred = readout - jnp.mean(readout, axis=-1, keepdims=True)
    normed = centred * lax.rsqrt(jnp.mean(centred * centred, axis=-1, keepdims=True) + EPS)
    normed = normed * scales.astype(jnp.float32).reshape(head_count, head_dim)
    gated_out = normed.reshape(row_count, head_count * head_dim) * jax.nn.silu(
        gate_pre.astype(jnp.float32)
    )
    return (gated_out.astype(jnp.bfloat16), new_state)


def slot_of(route_ids, expert_count, capacity):
    flat_ids = route_ids.reshape(-1)
    onehot = (flat_ids[:, None] == jnp.arange(expert_count, dtype=jnp.int32)[None, :]).astype(
        jnp.int32
    )
    ranking = jnp.sum((jnp.cumsum(onehot, axis=0) - 1) * onehot, axis=1)
    return flat_ids * capacity + ranking


def on_device(
    inputs,
    positions,
    ret_state,
    norm_mix,
    w_query,
    w_key,
    w_value,
    w_gate_in,
    head_gain,
    w_out,
    norm_ffn,
    route_ids,
    route_weight,
    exp_gate,
    exp_up,
    exp_down,
    dense_gate,
    dense_up,
    dense_down,
    branch_gate,
):
    seq_count = inputs.shape[0]
    top_count = route_ids.shape[1]
    ep_size = lax.axis_size("ep")
    local_experts = exp_gate.shape[0]
    expert_count = ep_size * local_experts
    capacity = max(2, 2 * seq_count * top_count // expert_count)
    normed = rms_scale(inputs, norm_mix)
    columns = lax.all_to_all(normed, "ep", split_axis=1, concat_axis=0, tiled=True)
    joined = jnp.concatenate([w_query, w_key, w_value, w_gate_in], axis=1)
    segment = columns
    summed = lax.psum_scatter(
        jnp.dot(segment, joined, preferred_element_type=jnp.float32),
        "ep",
        scatter_dimension=0,
        tiled=True,
    ).astype(jnp.bfloat16)
    queries, keys_new, values_new, gate_pre = jnp.split(summed, 4, axis=1)
    local_heads = ret_state.shape[1]
    log_gamma = lax.dynamic_slice_in_dim(
        log_decay(HEADS), lax.axis_index("tp") * local_heads, local_heads
    )
    retained, new_state = retain(
        queries, keys_new, values_new, gate_pre, ret_state, positions, head_gain, log_gamma
    )
    partial_cols = jnp.dot(
        lax.all_gather(retained, "ep", axis=0, tiled=True),
        w_out,
        preferred_element_type=jnp.float32,
    )
    rounded = lax.optimization_barrier(partial_cols.astype(jnp.bfloat16)).astype(jnp.float32)
    mixer_cols = lax.psum(rounded.astype(jnp.bfloat16), "tp")
    mixer_out = lax.all_to_all(mixer_cols, "ep", split_axis=0, concat_axis=1, tiled=True)
    residual_sum = (inputs.astype(jnp.float32) + mixer_out.astype(jnp.float32)).astype(jnp.bfloat16)
    normed_ffn = rms_scale(residual_sum, norm_ffn)
    slot_index = slot_of(route_ids, expert_count, capacity)
    slot_total = expert_count * capacity
    placing = (jnp.arange(slot_total, dtype=jnp.int32)[:, None] == slot_index[None, :]).astype(
        jnp.float32
    )
    by_token = jnp.sum(placing.reshape(slot_total, seq_count, top_count), axis=2)
    outgoing = (
        jnp.dot(by_token.astype(jnp.bfloat16), normed_ffn, preferred_element_type=jnp.float32)
        .astype(jnp.bfloat16)
        .reshape(expert_count, capacity, D)
    )
    received = lax.all_to_all(outgoing, "ep", split_axis=0, concat_axis=0, tiled=True)
    slot_count = received.shape[1]
    grouped = received.reshape(ep_size, local_experts, slot_count, D)
    gate_part = jnp.einsum("sjnd,jdf->sjnf", grouped, exp_gate, preferred_element_type=jnp.float32)
    up_part = jnp.einsum("sjnd,jdf->sjnf", grouped, exp_up, preferred_element_type=jnp.float32)
    hidden = (jax.nn.silu(gate_part) * up_part).astype(jnp.bfloat16)
    partial_out = jnp.einsum(
        "sjnf,jfd->sjnd", hidden, exp_down, preferred_element_type=jnp.float32
    ).reshape(received.shape[0], slot_count, D)
    returned = lax.all_to_all(
        partial_out.astype(jnp.bfloat16), "ep", split_axis=0, concat_axis=0, tiled=True
    ).astype(partial_out.dtype)
    widened = route_weight.astype(jnp.float32)
    share_flat = (widened / jnp.sum(widened, axis=-1, keepdims=True)).reshape(-1)
    weighting = jnp.sum(
        (placing * share_flat[None, :]).reshape(slot_total, seq_count, top_count), axis=2
    )
    expert_part = jnp.einsum(
        "rt,rd->td", weighting, returned.reshape(slot_total, D), precision=lax.Precision.HIGHEST
    )
    segment = lax.all_gather(normed_ffn, "ep", axis=0, tiled=True)
    gate_part = jnp.dot(segment, dense_gate, preferred_element_type=jnp.float32)
    up_part = jnp.dot(segment, dense_up, preferred_element_type=jnp.float32)
    hidden = (jax.nn.silu(gate_part) * up_part).astype(jnp.bfloat16)
    opening = jax.nn.sigmoid(
        jnp.dot(segment, branch_gate[:, None], preferred_element_type=jnp.float32)
    )
    branch_term = jnp.dot(hidden, dense_down, preferred_element_type=jnp.float32) * opening
    summed_branch = lax.psum_scatter(branch_term, "ep", scatter_dimension=0, tiled=True)
    summed_branch = summed_branch + expert_part
    width_total = lax.psum(summed_branch.astype(jnp.bfloat16), "tp").astype(jnp.float32)
    layer_out = (residual_sum.astype(jnp.float32) + width_total).astype(jnp.bfloat16)
    return (layer_out, new_state)


def solution(mesh):
    in_specs = (
        P("ep", None),
        P("ep"),
        P("ep", "tp", None, None),
        P(),
        P("ep", "tp"),
        P("ep", "tp"),
        P("ep", "tp"),
        P("ep", "tp"),
        P("tp"),
        P("tp", "ep"),
        P(),
        P("ep", None),
        P("ep", None),
        P("ep", None, "tp"),
        P("ep", None, "tp"),
        P("ep", "tp", None),
        P(None, ("ep", "tp")),
        P(None, ("ep", "tp")),
        P(("ep", "tp"), None),
        P(),
    )
    out_specs = (P("ep", None), P("ep", "tp", None, None))
    return jax.shard_map(
        on_device, mesh=mesh, in_specs=in_specs, out_specs=out_specs, check_vma=False
    )
```

profile of v0, /device:TPU:0, one launch (start us, length us, event | category | flops | bytes accessed | tf_op | source)
XLA Modules:
  0.0 408.9 jit_solution(14892159099410248619)
XLA Ops:
  7.2 0.8 convert_element_type.89
  8.1 1.0 fusion.39
  9.0 0.9 copy_bitcast_fusion
  10.0 15.7 %all_to_all.42 = bf16[16,16,128]{2,0,1:T(8,128)(2,1)S(1)} all-to-all(bf16[16,16,128]{2,0,1:T(8,128)(2,1)S(1)} %copy_bitcast_fusion), channel_id=1, replica_groups=mesh['ep'=16,'tp'=2] {'ep'}, dimensions={1} | all-to-all | bytes 131072 | tf_op jit(solution)/shard_map/all_to_all | solution.py:101
  25.6 3.4 fusion.25
  29.1 0.0 all-reduce.3.cloned.1.call-start
  29.2 0.6 copy-done.11
  29.8 0.1 dynamic-slice_exponential_fusion
  29.9 0.1 multiply_cosine_fusion
  30.0 128.4 %reduce-scatter.3.cloned.1.call-done = f32[16,3072]{1,0:T(8,128)} async-done(((f32[256,3072]{1,0:T(8,128)}), f32[16,3072]{1,0:T(8,128)}) %reduce-scatter.3.cloned.1.call-update) | async-done | bytes 196624 | tf_op jit(solution)/shard_map/reduce_scatter | solution.py:104
  158.3 0.9 convert_element_type.91
  159.4 0.1 multiply_subtract_fusion.1
  159.5 0.1 maximum_multiply_fusion
  159.6 0.1 maximum_bitcast_fusion
  159.7 4.5 %multiply_add_fusion = f32[16,6,128,128]{3,2,1,0:T(8,128)S(1)} fusion(f32[16,6,128,128]{3,2,1,0:T(8,128)} %param.22, f32[16,6,128]{2,1,0:T(8,128)S(1)} %reshape.211, f32[16,6,128]{2,1,0:T(8,128)S(1)} %maximum_multiply_fusion, f32[6]{0:T(128)S(1)} %dynamic-slice_exponential_fusion), kind=kLoop, calls=%fused_computation | loop fusion | flops 4718592 | bytes 12681240 | tf_op jit(solution)/shard_map/add | solution.py:50
  164.2 5.5 %fusion.63 = f32[16,6,1,128]{3,2,1,0:T(1,128)S(1)} fusion(f32[16,6,128,128]{3,2,1,0:T(8,128)S(1)} %multiply_add_fusion, f32[16,6,128,1]{2,1,0,3:T(8,128)S(1)} %maximum_bitcast_fusion), kind=kOutput, calls=%fused_computation.76 | convolution fusion | flops 18874368 | bytes 6389760 | tf_op jit(solution)/shard_map/shd,shdv->shv/dot_general | solution.py:53
  169.6 0.1 bitcast_reduce_fusion
  169.7 0.2 fusion.56
  169.9 0.1 fusion.57
  170.1 40.8 %all_gather.6 = bf16[256,768]{1,0:T(8,128)(2,1)S(1)} all-gather(bf16[16,768]{1,0:T(8,128)(2,1)S(1)} %fusion.65), channel_id=1, replica_groups=mesh['ep'=16,'tp'=2] {'ep'}, dimensions={0}, use_global_device_ids=true | all-gather | bytes 417792 | tf_op jit(solution)/shard_map/all_gather | solution.py:119
  210.9 0.9 convolution_convert_fusion.2
  211.8 13.7 %all-reduce.3.cloned.1.call-done = bf16[16,16,128]{2,1,0:T(8,128)(2,1)} async-done(((bf16[16,16,128]{2,1,0:T(8,128)(2,1)}), bf16[16,16,128]{2,1,0:T(8,128)(2,1)}) %all-reduce.3.cloned.1.call-update) | async-done | bytes 65552 | tf_op jit(solution)/shard_map/psum | solution.py:124
  225.5 6.8 %all-to-all-start.1 = ((bf16[16,16,128]{2,1,0:T(8,128)(2,1)}), bf16[16,16,128]{2,1,0:T(8,128)(2,1)S(1)}, u32[]{:S(2)}, u32[]{:S(2)}) async-start(bf16[16,16,128]{2,1,0:T(8,128)(2,1)} %all-reduce.3.cloned.1.call-done), calls=%async_computation.2 | async-start | bytes 131072 | tf_op jit(solution)/shard_map/all_to_all | solution.py:125
  232.4 7.5 %all-to-all-done.1 = bf16[16,16,128]{2,1,0:T(8,128)(2,1)S(1)} async-done(((bf16[16,16,128]{2,1,0:T(8,128)(2,1)}), bf16[16,16,128]{2,1,0:T(8,128)(2,1)S(1)}, u32[]{:S(2)}, u32[]{:S(2)}) %all-to-all-start.1) | async-done | bytes 65568 | tf_op jit(solution)/shard_map/all_to_all | solution.py:125
  239.9 0.1 fusion.43
  240.0 0.7 fusion.45
  240.9 52.0 %all-gather.2.cloned.1.call-done = bf16[256,2048]{1,0:T(8,128)(2,1)} async-done(((bf16[16,2048]{1,0:T(8,128)(2,1)}), bf16[256,2048]{1,0:T(8,128)(2,1)}) %all-gather.2.cloned.1.call-update) | async-done | bytes 1048592 | tf_op jit(solution)/shard_map/all_gather | solution.py:159
  292.9 1.7 fusion.73
  294.6 1.8 fusion.72
  296.4 3.3 convolution_multiply_fusion
  299.8 0.6 copy-done.6
  300.4 0.1 copy.38
  300.5 0.1 eq.31
  300.6 0.1 fusion.66
  300.7 0.1 reduce_window_sum.11
  300.8 0.2 select_reduce_fusion.1
  301.0 0.1 reduce_sum.79
  301.1 0.1 copy.39
  301.2 0.1 convert_reduce_fusion
  301.3 0.3 fusion
  301.6 21.7 %all_to_all.43 = bf16[16,8,2048]{2,1,0:T(8,128)(2,1)S(1)} all-to-all(bf16[16,8,2048]{2,1,0:T(8,128)(2,1)S(1)} %fusion), channel_id=1, replica_groups=mesh['ep'=16,'tp'=2] {'ep'}, dimensions={0} | all-to-all | bytes 1048576 | tf_op jit(solution)/shard_map/all_to_all | solution.py:139
  323.3 2.0 fusion.7
  325.3 2.4 convolution_convert_fusion
  327.8 21.4 %all_to_all.44 = bf16[16,8,2048]{2,1,0:T(8,128)(2,1)S(1)} all-to-all(bf16[16,8,2048]{2,1,0:T(8,128)(2,1)S(1)} %convolution_convert_fusion), channel_id=1, replica_groups=mesh['ep'=16,'tp'=2] {'ep'}, dimensions={0} | all-to-all | bytes 1048576 | tf_op jit(solution)/shard_map/all_to_all | solution.py:148
  349.2 33.9 %reduce-scatter.5.cloned.1.call-done = f32[16,2048]{1,0:T(8,128)} async-done(((f32[256,2048]{1,0:T(8,128)}), f32[16,2048]{1,0:T(8,128)}) %reduce-scatter.5.cloned.1.call-update) | async-done | bytes 131088 | tf_op jit(solution)/shard_map/reduce_scatter | solution.py:167
  383.1 1.9 fusion.1
  385.0 15.9 %all-reduce.5.cloned.1.call-done = bf16[16,2048]{1,0:T(8,128)(2,1)} async-done(((bf16[16,2048]{1,0:T(8,128)(2,1)}), bf16[16,2048]{1,0:T(8,128)(2,1)}) %all-reduce.5.cloned.1.call-update) | async-done | bytes 65552 | tf_op jit(solution)/shard_map/psum | solution.py:169
  400.9 1.5 fusion.46
  (50 shorter events, 0.5 us)
Async XLA Ops:
  7.2 318.2 %copy-start = (bf16[1,512,2048]{2,1,0:T(8,128)(2,1)S(1)}, bf16[1,512,2048]{2,1,0:T(8,128)(2,1)}, u32[]{:S(2)}) copy-start(bf16[1,512,2048]{2,1,0:T(8,128)(2,1)} %param.35) | copy-start | bytes 6291460
  7.2 151.2 %reduce-scatter.3.cloned.1.call-start = ((), (), s32[]{:S(2)}) async-start(), calls=%async_computation.6 | async-start | bytes 3342336 | tf_op jit(solution)/shard_map/reduce_scatter | solution.py:104
  29.1 0.7 copy-start.11
  29.1 0.8 copy-start.9
  29.1 196.4 %all-reduce.3.cloned.1.call-start = ((), (), s32[]{:S(2)}) async-start(), calls=%async_computation.7 | async-start | bytes 131072 | tf_op jit(solution)/shard_map/psum | solution.py:124
  164.1 5.5 %copy-start.1 = (f32[16,6,128,128]{3,2,1,0:T(8,128)}, f32[16,6,128,128]{3,2,1,0:T(8,128)S(1)}, u32[]{:S(2)}) copy-start(f32[16,6,128,128]{3,2,1,0:T(8,128)S(1)} %multiply_add_fusion) | copy-start | bytes 18874372
  164.1 46.7 %copy-start.5 = (bf16[768,128]{1,0:T(8,128)(2,1)S(1)}, bf16[768,128]{1,0:T(8,128)(2,1)}, u32[]{:S(2)}) copy-start(bf16[768,128]{1,0:T(8,128)(2,1)} %param.29) | copy-start | bytes 589828
  164.1 68.3 %copy-start.7 = (bf16[2048]{0:T(1024)(128)(2,1)S(1)}, bf16[2048]{0:T(1024)(128)(2,1)}, u32[]{:S(2)}) copy-start(bf16[2048]{0:T(1024)(128)(2,1)} %param.30) | copy-start | bytes 12292
  164.2 75.7 %copy-start.3 = (bf16[16,2048]{1,0:T(8,128)(2,1)S(1)}, bf16[16,2048]{1,0:T(8,128)(2,1)}, u32[]{:S(2)}) copy-start(bf16[16,2048]{1,0:T(8,128)(2,1)} %param.20) | copy-start | bytes 196612
  169.6 71.2 %copy-start.8 = (bf16[2048]{0:T(1024)(128)(2,1)S(1)}, bf16[2048]{0:T(1024)(128)(2,1)}, u32[]{:S(2)}) copy-start(bf16[2048]{0:T(1024)(128)(2,1)} %param.39) | copy-start | bytes 12292
  225.5 14.4 %all-to-all-start.1 = ((bf16[16,16,128]{2,1,0:T(8,128)(2,1)}), bf16[16,16,128]{2,1,0:T(8,128)(2,1)S(1)}, u32[]{:S(2)}, u32[]{:S(2)}) async-start(bf16[16,16,128]{2,1,0:T(8,128)(2,1)} %all-reduce.3.cloned.1.call-done), calls=%async_computation.2 | async-start | bytes 131072 | tf_op jit(solution)/shard_map/all_to_all | solution.py:125
  232.4 60.6 %all-gather.2.cloned.1.call-start = ((), (), s32[]{:S(2)}) async-start(), calls=%async_computation.8 | async-start | bytes 1114112 | tf_op jit(solution)/shard_map/all_gather | solution.py:159
  240.8 142.3 %reduce-scatter.5.cloned.1.call-start = ((), (), s32[]{:S(2)}) async-start(), calls=%async_computation.9 | async-start | bytes 2228224 | tf_op jit(solution)/shard_map/reduce_scatter | solution.py:167
  292.9 3.5 copy-start.2
  299.8 0.7 copy-start.6
  299.8 1.4 copy-start.10
  299.8 1.5 copy-start.4
  299.8 101.1 %all-reduce.5.cloned.1.call-start = ((), (), s32[]{:S(2)}) async-start(), calls=%async_computation.10 | async-start | bytes 131072 | tf_op jit(solution)/shard_map/psum | solution.py:169
Sparse Core Ops, SparseCore 0:
  29.2 129.0 reduce-scatter.2
  211.9 13.5 all-reduce.2
  240.9 51.9 all-gather.1
  299.9 83.1 reduce-scatter.4
  385.8 15.0 all-reduce.4
where the time goes:
time: 410 us; the launch traced here: 409 us
  waiting for transfers between devices  251 us (61%)
  blocking collectives  99.6 us (24%)
  matrix products  23.2 us (6%)
  between operations  14.1 us (3%)
  other arithmetic  11.8 us (3%)
  starting transfers between devices  7.03 us (2%)
    reduce_scatter x1, waiting for transfers between devices, on_device(): lax.psum_scatter(jnp.dot(segment, joined, preferred_element_type=jnp.floa...  128 us
    all_gather x1, waiting for transfers between devices, on_device(): segment = lax.all_gather(normed_ffn, 'ep', axis=0, tiled=True)  52 us
    all_gather x1, blocking collectives, on_device(): lax.all_gather(retained, 'ep', axis=0, tiled=True)  40.8 us
    reduce_scatter x1, waiting for transfers between devices, on_device(): lax.psum_scatter(branch_term, 'ep', scatter_dimension=0, tiled=True)  33.9 us
    all_to_all x1, blocking collectives, on_device(): lax.all_to_all(outgoing, 'ep', split_axis=0, concat_axis=0, tiled=True)  21.7 us
    all_to_all x1, blocking collectives, on_device(): lax.all_to_all(partial_out.astype(jnp.bfloat16), 'ep', split_axis=0, conc...  21.4 us
    psum x1, waiting for transfers between devices, on_device(): lax.psum(summed_branch.astype(jnp.bfloat16), 'tp').astype(jnp.float32)  15.9 us
    all_to_all x1, blocking collectives, on_device(): lax.all_to_all(normed, 'ep', split_axis=1, concat_axis=0, tiled=True)  15.7 us
  transfers between devices with their start and end apart: 6, of which 6 were waited for; matrix products, arithmetic and copies ran while one was open for 1% of the time, Pallas kernels for 0%

commit v1 on v0

--- a/solution.py
+++ b/solution.py
@@ -116,7 +116,15 @@
         queries, keys_new, values_new, gate_pre, ret_state, positions, head_gain, log_gamma
     )
     partial_cols = jnp.dot(
-        lax.all_gather(retained, "ep", axis=0, tiled=True),
+        jnp.concatenate(
+            jax.lax.all_to_all(
+                jnp.stack([retained for _ in range(jax.lax.axis_size("ep"))]),
+                axis_name="ep",
+                split_axis=0,
+                concat_axis=0,
+            ),
+            axis=0,
+        ),
         w_out,
         preferred_element_type=jnp.float32,
     )

time: 410 us -> 387 us (0.944)
  blocking collectives: 99.6 us -> 74.4 us
    all_gather x1 -> x0, blocking collectives: 40.8 us -> none  [on_device(): lax.all_gather(retained, 'ep', axis=0, tiled=True)]
    all_to_all x0 -> x1, blocking collectives: none -> 15.6 us  [on_device(): jax.lax.all_to_all(jnp.stack([retained for _ in range(jax.lax.axis_size('...]
  transfers between devices with their start and end apart: 6 -> 6, of which waited for: 6 -> 6; matrix products, arithmetic and copies ran while one was open for 1% -> 2% of each run, Pallas kernels for 0% -> 0%
where the time goes in v1:
time: 387 us; the launch traced here: 386 us
  waiting for transfers between devices  254 us (66%)
  blocking collectives  74.4 us (19%)
  matrix products  23.2 us (6%)
  between operations  14.1 us (4%)
  other arithmetic  11.8 us (3%)
  starting transfers between devices  7.03 us (2%)
    reduce_scatter x1, waiting for transfers between devices, on_device(): lax.psum_scatter(jnp.dot(segment, joined, preferred_element_type=jnp.floa...  128 us
    all_gather x1, waiting for transfers between devices, on_device(): segment = lax.all_gather(normed_ffn, 'ep', axis=0, tiled=True)  52 us
    reduce_scatter x1, waiting for transfers between devices, on_device(): lax.psum_scatter(branch_term, 'ep', scatter_dimension=0, tiled=True)  33.8 us
    all_to_all x1, blocking collectives, on_device(): lax.all_to_all(outgoing, 'ep', split_axis=0, concat_axis=0, tiled=True)  21.7 us
    all_to_all x1, blocking collectives, on_device(): lax.all_to_all(partial_out.astype(jnp.bfloat16), 'ep', split_axis=0, conc...  21.5 us
    psum x1, waiting for transfers between devices, on_device(): lax.psum(summed_branch.astype(jnp.bfloat16), 'tp').astype(jnp.float32)  16.5 us
    psum x1, waiting for transfers between devices, on_device(): mixer_cols = lax.psum(rounded.astype(jnp.bfloat16), 'tp')  15.9 us
    all_to_all x1, blocking collectives, on_device(): lax.all_to_all(normed, 'ep', split_axis=1, concat_axis=0, tiled=True)  15.7 us
  transfers between devices with their start and end apart: 6, of which 6 were waited for; matrix products, arithmetic and copies ran while one was open for 2% of the time, Pallas kernels for 0%

profile of v1, /device:TPU:0, one launch (start us, length us, event | category | flops | bytes accessed | tf_op | source)
XLA Modules:
  0.0 386.4 jit_solution(11307829802066298847)
XLA Ops:
  7.2 0.8 convert_element_type.89
  8.1 1.0 fusion.39
  9.0 0.9 copy_bitcast_fusion
  10.0 15.7 %all_to_all.47 = bf16[16,16,128]{2,0,1:T(8,128)(2,1)S(1)} all-to-all(bf16[16,16,128]{2,0,1:T(8,128)(2,1)S(1)} %copy_bitcast_fusion), channel_id=1, replica_groups=mesh['ep'=16,'tp'=2] {'ep'}, dimensions={1} | all-to-all | bytes 131072 | tf_op jit(solution)/shard_map/all_to_all | solution.py:101
  25.6 3.4 fusion.25
  29.2 0.6 copy-done.11
  29.8 0.1 dynamic-slice_exponential_fusion
  29.9 0.1 multiply_cosine_fusion
  30.0 128.4 %reduce-scatter.3.cloned.1.call-done = f32[16,3072]{1,0:T(8,128)} async-done(((f32[256,3072]{1,0:T(8,128)}), f32[16,3072]{1,0:T(8,128)}) %reduce-scatter.3.cloned.1.call-update) | async-done | bytes 196624 | tf_op jit(solution)/shard_map/reduce_scatter | solution.py:104
  158.3 0.9 convert_element_type.91
  159.4 0.1 multiply_subtract_fusion.1
  159.5 0.1 maximum_multiply_fusion
  159.6 0.1 maximum_bitcast_fusion
  159.7 4.5 %multiply_add_fusion = f32[16,6,128,128]{3,2,1,0:T(8,128)S(1)} fusion(f32[16,6,128,128]{3,2,1,0:T(8,128)} %param.22, f32[16,6,128]{2,1,0:T(8,128)S(1)} %reshape.217, f32[16,6,128]{2,1,0:T(8,128)S(1)} %maximum_multiply_fusion, f32[6]{0:T(128)S(1)} %dynamic-slice_exponential_fusion), kind=kLoop, calls=%fused_computation | loop fusion | flops 4718592 | bytes 12681240 | tf_op jit(solution)/shard_map/add | solution.py:50
  164.1 5.5 %fusion.63 = f32[16,6,1,128]{3,2,1,0:T(1,128)S(1)} fusion(f32[16,6,128,128]{3,2,1,0:T(8,128)S(1)} %multiply_add_fusion, f32[16,6,128,1]{2,1,0,3:T(8,128)S(1)} %maximum_bitcast_fusion), kind=kOutput, calls=%fused_computation.76 | convolution fusion | flops 18874368 | bytes 6389760 | tf_op jit(solution)/shard_map/shd,shdv->shv/dot_general | solution.py:53
  169.6 0.1 bitcast_reduce_fusion
  169.7 0.2 fusion.56
  169.9 0.1 fusion.57
  170.1 15.6 %all_to_all.48 = bf16[16,16,768]{2,1,0:T(8,128)(2,1)S(1)} all-to-all(bf16[16,16,768]{2,1,0:T(8,128)(2,1)S(1)} %stack.2), channel_id=1, replica_groups=mesh['ep'=16,'tp'=2] {'ep'}, dimensions={0} | all-to-all | bytes 786432 | tf_op jit(solution)/shard_map/all_to_all | solution.py:120
  185.7 0.9 convolution_convert_fusion.2
  186.6 15.9 %all-reduce.3.cloned.1.call-done = bf16[16,16,128]{2,1,0:T(8,128)(2,1)} async-done(((bf16[16,16,128]{2,1,0:T(8,128)(2,1)}), bf16[16,16,128]{2,1,0:T(8,128)(2,1)}) %all-reduce.3.cloned.1.call-update) | async-done | bytes 65552 | tf_op jit(solution)/shard_map/psum | solution.py:132
  202.5 6.8 %all-to-all-start.2 = ((bf16[16,16,128]{2,1,0:T(8,128)(2,1)}), bf16[16,16,128]{2,1,0:T(8,128)(2,1)S(1)}, u32[]{:S(2)}, u32[]{:S(2)}) async-start(bf16[16,16,128]{2,1,0:T(8,128)(2,1)} %all-reduce.3.cloned.1.call-done), calls=%async_computation.3 | async-start | bytes 131072 | tf_op jit(solution)/shard_map/all_to_all | solution.py:133
  209.4 7.5 %all-to-all-done.2 = bf16[16,16,128]{2,1,0:T(8,128)(2,1)S(1)} async-done(((bf16[16,16,128]{2,1,0:T(8,128)(2,1)}), bf16[16,16,128]{2,1,0:T(8,128)(2,1)S(1)}, u32[]{:S(2)}, u32[]{:S(2)}) %all-to-all-start.2) | async-done | bytes 65568 | tf_op jit(solution)/shard_map/all_to_all | solution.py:133
  216.9 0.1 fusion.43
  217.0 0.7 fusion.45
  217.9 52.0 %all-gather.2.cloned.1.call-done = bf16[256,2048]{1,0:T(8,128)(2,1)} async-done(((bf16[16,2048]{1,0:T(8,128)(2,1)}), bf16[256,2048]{1,0:T(8,128)(2,1)}) %all-gather.2.cloned.1.call-update) | async-done | bytes 1048592 | tf_op jit(solution)/shard_map/all_gather | solution.py:167
  269.9 1.7 fusion.73
  271.6 1.8 fusion.72
  273.4 3.3 convolution_multiply_fusion
  276.8 0.0 all-reduce.5.cloned.1.call-start
  276.8 0.6 copy-done.6
  277.4 0.1 copy.38
  277.5 0.1 eq.31
  277.6 0.1 fusion.66
  277.7 0.1 reduce_window_sum.11
  277.8 0.2 select_reduce_fusion.1
  278.0 0.1 reduce_sum.79
  278.0 0.1 copy.39
  278.2 0.1 convert_reduce_fusion
  278.3 0.3 fusion
  278.6 21.7 %all_to_all.49 = bf16[16,8,2048]{2,1,0:T(8,128)(2,1)S(1)} all-to-all(bf16[16,8,2048]{2,1,0:T(8,128)(2,1)S(1)} %fusion), channel_id=1, replica_groups=mesh['ep'=16,'tp'=2] {'ep'}, dimensions={0} | all-to-all | bytes 1048576 | tf_op jit(solution)/shard_map/all_to_all | solution.py:147
  300.3 2.0 fusion.7
  302.3 2.4 convolution_convert_fusion
  304.8 21.5 %all_to_all.50 = bf16[16,8,2048]{2,1,0:T(8,128)(2,1)S(1)} all-to-all(bf16[16,8,2048]{2,1,0:T(8,128)(2,1)S(1)} %convolution_convert_fusion), channel_id=1, replica_groups=mesh['ep'=16,'tp'=2] {'ep'}, dimensions={0} | all-to-all | bytes 1048576 | tf_op jit(solution)/shard_map/all_to_all | solution.py:156
  326.2 33.8 %reduce-scatter.5.cloned.1.call-done = f32[16,2048]{1,0:T(8,128)} async-done(((f32[256,2048]{1,0:T(8,128)}), f32[16,2048]{1,0:T(8,128)}) %reduce-scatter.5.cloned.1.call-update) | async-done | bytes 131088 | tf_op jit(solution)/shard_map/reduce_scatter | solution.py:175
  360.0 1.9 fusion.1
  361.9 16.5 %all-reduce.5.cloned.1.call-done = bf16[16,2048]{1,0:T(8,128)(2,1)} async-done(((bf16[16,2048]{1,0:T(8,128)(2,1)}), bf16[16,2048]{1,0:T(8,128)(2,1)}) %all-reduce.5.cloned.1.call-update) | async-done | bytes 65552 | tf_op jit(solution)/shard_map/psum | solution.py:177
  378.4 1.5 fusion.46
  (51 shorter events, 0.5 us)
Async XLA Ops:
  7.2 295.2 %copy-start = (bf16[1,512,2048]{2,1,0:T(8,128)(2,1)S(1)}, bf16[1,512,2048]{2,1,0:T(8,128)(2,1)}, u32[]{:S(2)}) copy-start(bf16[1,512,2048]{2,1,0:T(8,128)(2,1)} %param.35) | copy-start | bytes 6291460
  7.2 151.2 %reduce-scatter.3.cloned.1.call-start = ((), (), s32[]{:S(2)}) async-start(), calls=%async_computation.7 | async-start | bytes 3342336 | tf_op jit(solution)/shard_map/reduce_scatter | solution.py:104
  29.1 0.7 copy-start.11
  29.1 0.8 copy-start.9
  29.1 173.4 %all-reduce.3.cloned.1.call-start = ((), (), s32[]{:S(2)}) async-start(), calls=%async_computation.8 | async-start | bytes 131072 | tf_op jit(solution)/shard_map/psum | solution.py:132
  164.1 5.5 %copy-start.1 = (f32[16,6,128,128]{3,2,1,0:T(8,128)}, f32[16,6,128,128]{3,2,1,0:T(8,128)S(1)}, u32[]{:S(2)}) copy-start(f32[16,6,128,128]{3,2,1,0:T(8,128)S(1)} %multiply_add_fusion) | copy-start | bytes 18874372
  164.1 21.6 %copy-start.5 = (bf16[768,128]{1,0:T(8,128)(2,1)S(1)}, bf16[768,128]{1,0:T(8,128)(2,1)}, u32[]{:S(2)}) copy-start(bf16[768,128]{1,0:T(8,128)(2,1)} %param.29) | copy-start | bytes 589828
  169.6 39.8 %copy-start.7 = (bf16[2048]{0:T(1024)(128)(2,1)S(1)}, bf16[2048]{0:T(1024)(128)(2,1)}, u32[]{:S(2)}) copy-start(bf16[2048]{0:T(1024)(128)(2,1)} %param.30) | copy-start | bytes 12292
  169.6 47.3 %copy-start.3 = (bf16[16,2048]{1,0:T(8,128)(2,1)S(1)}, bf16[16,2048]{1,0:T(8,128)(2,1)}, u32[]{:S(2)}) copy-start(bf16[16,2048]{1,0:T(8,128)(2,1)} %param.20) | copy-start | bytes 196612
  169.6 48.2 %copy-start.8 = (bf16[2048]{0:T(1024)(128)(2,1)S(1)}, bf16[2048]{0:T(1024)(128)(2,1)}, u32[]{:S(2)}) copy-start(bf16[2048]{0:T(1024)(128)(2,1)} %param.39) | copy-start | bytes 12292
  202.5 14.4 %all-to-all-start.2 = ((bf16[16,16,128]{2,1,0:T(8,128)(2,1)}), bf16[16,16,128]{2,1,0:T(8,128)(2,1)S(1)}, u32[]{:S(2)}, u32[]{:S(2)}) async-start(bf16[16,16,128]{2,1,0:T(8,128)(2,1)} %all-reduce.3.cloned.1.call-done), calls=%async_computation.3 | async-start | bytes 131072 | tf_op jit(solution)/shard_map/all_to_all | solution.py:133
  209.4 60.6 %all-gather.2.cloned.1.call-start = ((), (), s32[]{:S(2)}) async-start(), calls=%async_computation.9 | async-start | bytes 1114112 | tf_op jit(solution)/shard_map/all_gather | solution.py:167
  217.8 142.2 %reduce-scatter.5.cloned.1.call-start = ((), (), s32[]{:S(2)}) async-start(), calls=%async_computation.10 | async-start | bytes 2228224 | tf_op jit(solution)/shard_map/reduce_scatter | solution.py:175
  269.9 3.5 copy-start.2
  276.8 0.7 copy-start.6
  276.8 1.4 copy-start.10
  276.8 1.5 copy-start.4
  276.8 101.6 %all-reduce.5.cloned.1.call-start = ((), (), s32[]{:S(2)}) async-start(), calls=%async_computation.11 | async-start | bytes 131072 | tf_op jit(solution)/shard_map/psum | solution.py:177
Sparse Core Ops, SparseCore 0:
  29.2 129.0 reduce-scatter.2
  186.7 15.7 all-reduce.2
  217.9 51.9 all-gather.1
  276.9 83.0 reduce-scatter.4
  362.7 15.6 all-reduce.4
